TPU v7x, 256 devices: a whole 4x4x8 slice. The times are simulated.
256 devices in a mesh: rep: 2 (over z_hi), fs: 16 (over z_lo, x), tp: 8 (over y, core).
Axes of the slice: x: 4, y: 4, z: 8 (z_hi: 2, z_lo: 4; z = z_hi * 4 + z_lo), core: 2. Of those that a mesh axis runs over, the one named last changes fastest.
Arguments:
- stream: bfloat16 [32768, 2048], P(('rep', 'fs', 'tp')), may hold values from -6 to 6
- gate_weight: bfloat16 [2048, 2816], P('fs', 'tp'), may hold values from -0.125 to 0.125
- up_weight: bfloat16 [2048, 2816], P('fs', 'tp'), may hold values from -0.125 to 0.125
- down_weight: bfloat16 [2816, 2048], P('tp', 'fs'), may hold values from -0.21875 to 0.21875
- query_weight: bfloat16 [2048, 512], P('fs', 'tp'), may hold values from -0.125 to 0.125
- key_weight: bfloat16 [2048, 512], P('fs', 'tp'), may hold values from -0.125 to 0.125
- value_weight: bfloat16 [2048, 1024], P('fs', 'tp'), may hold values from -0.125 to 0.125
- outgate_weight: bfloat16 [2048, 1024], P('fs', 'tp'), may hold values from -0.125 to 0.125
- decay_down: bfloat16 [2048, 32], replicated, may hold values from -0.125 to 0.125
- decay_up: bfloat16 [32, 512], P(None, 'tp'), may hold values from -2 to 2
- decay_bias: float32 [512], P('tp'), may hold values from -0.5 to 7
- head_gain: float32 [128], replicated, may hold values from 0.1 to 1.9
- out_weight: bfloat16 [1024, 2048], P('tp', 'fs'), may hold values from -0.375 to 0.375
- norm_gain: float32 [3, 2048], replicated, may hold values from 0.1 to 1.9
Outputs:
- layer_out: bfloat16 [32768, 2048], P(('rep', 'fs', 'tp'))
All inputs are finite; a program needn't handle non-finite values.
Results may differ from a plain program's by a relative error of at most 0.015.
Values may be sent and summed in bfloat16 or wider, within the bound.
A program may use at most 128 MiB of HBM per device.

v0:
```python
import jax
import jax.numpy as jnp
from jax import lax
from jax.sharding import PartitionSpec as P

DK = 64
DV = 128
BLOCK = 64
RESIDUAL_SCALE = 2.0**0.5
BRANCH_SCALE = 0.5
NORM_EPS = 1e-05
HEAD_EPS = 0.01
GATE_DIVISOR = 16.0


def from_everyone(value, axis):
    copies = jnp.broadcast_to(value, (lax.axis_size(axis), *value.shape))
    return lax.all_to_all(copies, axis, split_axis=0, concat_axis=0, tiled=True)


def joined_along(pieces, dim):
    pieces = jnp.moveaxis(pieces, 0, dim)
    lengths = pieces.shape
    return pieces.reshape(*lengths[:dim], lengths[dim] * lengths[dim + 1], *lengths[dim + 2 :])


def gather_directly(value, axis, dim):
    pieces = from_everyone(value, axis)
    return joined_along(pieces, dim)


def side_by_side(arrays, axis, dim, along):
    widths = [a.shape[along] for a in arrays]
    both = jnp.concatenate(arrays, axis=along)
    result = lax.all_gather(both, axis, axis=dim, tiled=True)
    return tuple(jnp.split(result, [sum(widths[:k]) for k in range(1, len(widths))], axis=along))


def layer_norm(values, norm_scale):
    average = jnp.mean(values, -1, keepdims=True)
    centred = values - average
    spread = jnp.mean(centred * centred, -1, keepdims=True)
    return (centred * lax.rsqrt(spread + NORM_EPS) * norm_scale).astype(jnp.bfloat16)


def blocked_mixer(query, key_rows, value_rows, log_gate):
    length, head_count, key_dim = query.shape
    value_dim = value_rows.shape[2]
    block_count = length // BLOCK

    def split_blocks(values):
        return values.reshape(block_count, BLOCK, head_count, values.shape[2]).transpose(0, 2, 1, 3)

    causal = jnp.tril(jnp.ones((BLOCK, BLOCK), dtype=bool))

    def advance(carried, inputs):
        query_blk, key_blk, value_blk, decay_blk = inputs
        log_gaps = decay_blk[:, :, None, :] - decay_blk[:, None, :, :]
        log_gaps = jnp.where(causal[None, :, :, None], log_gaps, -jnp.inf)
        scores = jnp.sum(
            query_blk[:, :, None, :] * key_blk[:, None, :, :] * jnp.exp(log_gaps), axis=-1
        )
        inside = jnp.einsum("hij,hjv->hiv", scores, value_blk)
        carried_part = jnp.einsum("hid,hdv->hiv", query_blk * jnp.exp(decay_blk), carried)
        closing = decay_blk[:, -1, :]
        update = jnp.einsum(
            "hjd,hjv->hdv", key_blk * jnp.exp(closing[:, None, :] - decay_blk), value_blk
        )
        return (carried * jnp.exp(closing)[:, :, None] + update, inside + carried_part)

    cumulative = jnp.cumsum(split_blocks(log_gate), axis=2)
    start_state = jnp.zeros((head_count, key_dim, value_dim), jnp.float32)
    _, outputs = lax.scan(
        advance,
        start_state,
        (split_blocks(query), split_blocks(key_rows), split_blocks(value_rows), cumulative),
    )
    return outputs.transpose(0, 2, 1, 3).reshape(length, head_count, value_dim)


def on_device(
    stream,
    gate_weight,
    up_weight,
    down_weight,
    query_weight,
    key_weight,
    value_weight,
    outgate_weight,
    decay_down,
    decay_up,
    decay_bias,
    head_gain,
    out_weight,
    norm_gain,
):
    down_local = gather_directly(down_weight, "fs", 1)
    down_full = lax.all_gather(down_local, "tp", axis=0, tiled=True)

    def ffn_half(current, norm_scale):
        gathered = lax.all_gather(current, "tp", axis=0, tiled=True)
        pieces = side_by_side((gate_weight, up_weight), "fs", 0, 1)
        gate = jnp.dot(gathered, pieces[0], preferred_element_type=jnp.float32)
        upward = jnp.dot(gathered, pieces[1], preferred_element_type=jnp.float32)
        hidden = (jax.nn.silu(gate) * upward).astype(jnp.bfloat16)
        own_hidden = lax.all_to_all(hidden, "tp", split_axis=0, concat_axis=1, tiled=True)
        summed = jnp.dot(own_hidden, down_full, preferred_element_type=jnp.float32)
        return layer_norm(
            RESIDUAL_SCALE * current.astype(jnp.float32) + BRANCH_SCALE * summed, norm_scale
        )

    first = ffn_half(stream, norm_gain[0])
    gathered = lax.all_gather(first, "tp", axis=0, tiled=True)
    length = gathered.shape[0]
    pieces = side_by_side((query_weight, key_weight, value_weight, outgate_weight), "fs", 0, 1)
    query, key_rows, value_rows, outgate = tuple(
        (jnp.dot(gathered, piece, preferred_element_type=jnp.float32) for piece in pieces)
    )
    query = query.astype(jnp.bfloat16)
    key_rows = key_rows.astype(jnp.bfloat16)
    value_rows = value_rows.astype(jnp.bfloat16)
    outgate = outgate.astype(jnp.bfloat16)
    low_rank = jnp.dot(gathered, decay_down, preferred_element_type=jnp.float32).astype(
        jnp.bfloat16
    )
    pre_gate = jnp.dot(low_rank, decay_up, preferred_element_type=jnp.float32) + decay_bias
    log_gate = jax.nn.log_sigmoid(pre_gate) / GATE_DIVISOR
    local_heads = query.shape[1] // DK
    mixed = blocked_mixer(
        query.astype(jnp.float32).reshape(length, local_heads, DK) * DK ** (-0.5),
        key_rows.astype(jnp.float32).reshape(length, local_heads, DK),
        value_rows.astype(jnp.float32).reshape(length, local_heads, DV),
        log_gate.reshape(length, local_heads, DK),
    )
    normed = mixed * lax.rsqrt(jnp.mean(mixed * mixed, -1, keepdims=True) + HEAD_EPS) * head_gain
    gated = (
        normed.reshape(length, local_heads * DV) * jax.nn.silu(outgate.astype(jnp.float32))
    ).astype(jnp.bfloat16)
    out_local = gather_directly(out_weight, "fs", 1)
    out_full = lax.all_gather(out_local, "tp", axis=0, tiled=True)
    own_gated = lax.all_to_all(gated, "tp", split_axis=0, concat_axis=1, tiled=True)
    summed = jnp.dot(own_gated, out_full, preferred_element_type=jnp.float32)
    second = layer_norm(RESIDUAL_SCALE * first.astype(jnp.float32) + summed, norm_gain[1])
    return ffn_half(second, norm_gain[2])


def solution(mesh):
    in_specs = (
        P(("rep", "fs", "tp"), None),
        P("fs", "tp"),
        P("fs", "tp"),
        P("tp", "fs"),
        P("fs", "tp"),
        P("fs", "tp"),
        P("fs", "tp"),
        P("fs", "tp"),
        P(),
        P(None, "tp"),
        P("tp"),
        P(),
        P("tp", "fs"),
        P(),
    )
    out_specs = P(("rep", "fs", "tp"), None)
    return jax.shard_map(
        on_device, mesh=mesh, in_specs=in_specs, out_specs=out_specs, check_vma=False
    )
```

profile of v0, /device:TPU:1, one launch (start us, length us, event | category | flops | bytes accessed | tf_op | source)
XLA Modules:
  0.0 473.2 jit_solution(7399616951409170826)
XLA Ops:
  6.5 1.7 pad_maximum_fusion
  8.3 0.7 all-gather.10.cloned.1.call-update
  9.0 1.1 broadcast_in_dim.32
  10.1 57.1 %all_to_all.67 = bf16[16,352,128]{2,1,0:T(8,128)(2,1)S(1)} all-to-all(bf16[16,352,128]{2,1,0:T(8,128)(2,1)S(1)} %broadcast_in_dim.32), channel_id=1, replica_groups=mesh['rep'=2,'fs'=16,'tp'=8] {'fs'}, dimensions={0} | all-to-all | bytes 2883584 | tf_op jit(solution)/shard_map/all_to_all | solution.py:18
  67.2 1.3 copy_bitcast_fusion
  68.9 0.7 pad_maximum_fusion.1
  69.6 27.4 %all-gather.8.cloned.1.call-done = bf16[2048,704]{0,1:T(8,128)(2,1)} async-done(((bf16[128,704]{0,1:T(8,128)(2,1)}), bf16[2048,704]{0,1:T(8,128)(2,1)}) %all-gather.8.cloned.1.call-update) | async-done | bytes 2883600 | tf_op jit(solution)/shard_map/all_gather | solution.py:35
  97.0 44.9 %all-gather.10.cloned.1.call-done = bf16[1024,2048]{1,0:T(8,128)(2,1)} async-done(((bf16[128,2048]{1,0:T(8,128)(2,1)}), bf16[1024,2048]{1,0:T(8,128)(2,1)}) %all-gather.10.cloned.1.call-update) | async-done | bytes 4194320 | tf_op jit(solution)/shard_map/all_gather | solution.py:101
  141.9 4.5 convolution_bitcast_fusion.2
  146.4 1.9 fusion.35
  148.3 1.0 copy.67
  149.3 3.7 all-to-all-start
  153.1 14.9 %all-to-all-done = bf16[8,128,352]{1,2,0:T(8,128)(2,1)S(1)} async-done(((bf16[8,128,352]{1,2,0:T(8,128)(2,1)}), bf16[8,128,352]{1,2,0:T(8,128)(2,1)S(1)}, u32[]{:S(2)}, u32[]{:S(2)}) %all-to-all-start) | async-done | bytes 720928 | tf_op jit(solution)/shard_map/all_to_all | solution.py:106
  168.0 45.3 %all-gather.12.cloned.1.call-done = bf16[2816,2048]{1,0:T(8,128)(2,1)} async-done(((bf16[352,2048]{1,0:T(8,128)(2,1)}), bf16[2816,2048]{1,0:T(8,128)(2,1)}) %all-gather.12.cloned.1.call-update) | async-done | bytes 11534352 | tf_op jit(solution)/shard_map/all_gather | solution.py:98
  213.3 6.0 %fusion.58 = (f32[128]{0:T(128)S(1)}, f32[128,2048]{1,0:T(8,128)S(1)}) fusion(bf16[128,2816]{0,1:T(8,128)(2,1)S(1)} %bitcast.148, bf16[2816,2048]{1,0:T(8,128)(2,1)} %all-gather.12.cloned.1.call-done, bf16[128,2048]{1,0:T(8,128)(2,1)S(1)} %copy-done.3), kind=kOutput, calls=%fused_computation.96 | convolution fusion | flops 1477705600 | bytes 13828608 | tf_op jit(solution)/shard_map/dot_general | solution.py:107
  219.3 0.3 multiply_reduce_fusion.3
  219.6 1.0 multiply_convert_fusion.2
  220.8 0.9 broadcast_in_dim.35
  221.7 7.0 %all-to-all-start.3 = ((bf16[16,128,128]{1,2,0:T(8,128)(2,1)}), bf16[16,128,128]{1,2,0:T(8,128)(2,1)S(1)}, u32[]{:S(2)}, u32[]{:S(2)}) async-start(bf16[16,128,128]{1,2,0:T(8,128)(2,1)} %broadcast_in_dim.35), calls=%async_computation.3 | async-start | bytes 1048576 | tf_op jit(solution)/shard_map/all_to_all | solution.py:18
  228.8 0.2 all-gather.18.cloned.1.call-start
  229.0 17.3 %all-to-all-done.3 = bf16[16,128,128]{1,2,0:T(8,128)(2,1)S(1)} async-done(((bf16[16,128,128]{1,2,0:T(8,128)(2,1)}), bf16[16,128,128]{1,2,0:T(8,128)(2,1)S(1)}, u32[]{:S(2)}, u32[]{:S(2)}) %all-to-all-start.3) | async-done | bytes 524320 | tf_op jit(solution)/shard_map/all_to_all | solution.py:18
  246.3 0.9 copy-done.4
  247.2 39.2 %all-gather.16.cloned.1.call-done = bf16[2048,384]{1,0:T(8,128)(2,1)} async-done(((bf16[128,384]{1,0:T(8,128)(2,1)}), bf16[2048,384]{1,0:T(8,128)(2,1)}) %all-gather.16.cloned.1.call-update) | async-done | bytes 1572880 | tf_op jit(solution)/shard_map/all_gather | solution.py:35
  286.4 45.3 %all-gather.14.cloned.1.call-done = bf16[1024,2048]{1,0:T(8,128)(2,1)} async-done(((bf16[128,2048]{1,0:T(8,128)(2,1)}), bf16[1024,2048]{1,0:T(8,128)(2,1)}) %all-gather.14.cloned.1.call-update) | async-done | bytes 4194320 | tf_op jit(solution)/shard_map/all_gather | solution.py:113
  331.8 3.8 fusion.45
  335.5 0.2 copy.57
  335.7 3.7 fusion.44
  339.5 0.2 copy.58
  339.7 3.8 fusion.56
  343.6 0.4 copy.47
  344.0 6.3 %fusion.61 = f32[16,1,64,64]{3,0,1,2:T(8,128)S(1)} fusion(f32[16,1,64,64]{3,0,1,2:T(8,128)S(1)} %copy.47), kind=kOutput, calls=%fused_computation.99 | output fusion | flops 4128768 | bytes 524288 | tf_op jit(solution)/shard_map/jit(cumsum)/reduce_window_sum | solution.py:71
  350.3 3.6 convolution_convert_fusion.1
  353.9 30.5 %while.13 = (s32[]{:T(128)}, f32[1,64,128]{2,1,0:T(8,128)S(1)}, f32[16,1,64,128]{3,2,1,0:T(8,128)S(1)}, f32[16,1,64,64]{3,0,1,2:T(8,128)S(1)}, f32[16,1,64,64]{3...) while((s32[]{:T(128)}, f32[1,64,128]{2,1,0:T(8,128)S(1)}, ...), condition=%wide.region_5.6_spmd.clone, body=%wide.region_3.5_spmd.clone.sunk | while | flops 4509699 | bytes 544884 | solution.py:73
  354.0 1.4 multiply_reduce_fusion.6
  355.9 1.4 multiply_reduce_fusion.6
  357.8 1.4 multiply_reduce_fusion.6
  359.7 1.4 multiply_reduce_fusion.6
  361.6 1.4 multiply_reduce_fusion.6
  363.5 1.4 multiply_reduce_fusion.6
  365.4 1.4 multiply_reduce_fusion.6
  367.3 1.4 multiply_reduce_fusion.6
  369.2 1.4 multiply_reduce_fusion.6
  371.1 1.4 multiply_reduce_fusion.6
  373.0 1.4 multiply_reduce_fusion.6
  374.9 1.4 multiply_reduce_fusion.6
  376.8 1.4 multiply_reduce_fusion.6
  378.7 1.4 multiply_reduce_fusion.6
  380.6 1.4 multiply_reduce_fusion.6
  382.6 1.4 multiply_reduce_fusion.6
  384.4 0.2 multiply_reduce_fusion.4
  384.7 3.6 fusion.52
  388.3 0.9 copy.54
  389.2 3.6 all-to-all-start.2
  392.8 6.5 %all-to-all-done.2 = bf16[8,128,128]{1,2,0:T(8,128)(2,1)S(1)} async-done(((bf16[8,128,128]{1,2,0:T(8,128)(2,1)}), bf16[8,128,128]{1,2,0:T(8,128)(2,1)S(1)}, u32[]{:S(2)}, u32[]{:S(2)}) %all-to-all-start.2) | async-done | bytes 262176 | tf_op jit(solution)/shard_map/all_to_all | solution.py:141
  399.3 3.8 fusion.59
  403.0 0.3 multiply_reduce_fusion.2
  403.3 1.0 multiply_convert_fusion.1
  404.4 35.0 %all-gather.20.cloned.1.call-done = bf16[1024,2048]{1,0:T(8,128)(2,1)} async-done(((bf16[128,2048]{1,0:T(8,128)(2,1)}), bf16[1024,2048]{1,0:T(8,128)(2,1)}) %all-gather.20.cloned.1.call-update) | async-done | bytes 4194320 | tf_op jit(solution)/shard_map/all_gather | solution.py:101
  439.3 4.5 fusion.38
  443.8 4.6 fusion.34
  448.6 14.7 %all_to_all.68 = bf16[8,128,352]{1,2,0:T(8,128)(2,1)S(1)} all-to-all(bf16[8,128,352]{1,2,0:T(8,128)(2,1)S(1)} %bitcast.150), channel_id=1, replica_groups=mesh['rep'=2,'fs'=16,'tp'=8] {'tp'}, dimensions={0} | all-to-all | bytes 1441792 | tf_op jit(solution)/shard_map/all_to_all | solution.py:106
  463.3 1.8 fusion.60
  465.1 0.3 multiply_reduce_fusion.1
  465.3 1.0 multiply_convert_fusion
  (195 shorter events, 9.2 us)
Async XLA Ops:
  6.5 333.1 %copy-start = (bf16[2048,32]{0,1:T(8,128)(2,1)S(1)}, bf16[2048,32]{0,1:T(8,128)(2,1)}, u32[]{:S(2)}) copy-start(bf16[2048,32]{0,1:T(8,128)(2,1)} %param.24) | copy-start | bytes 393220
  6.5 90.5 %all-gather.8.cloned.1.call-start = ((), (), s32[]{:S(2)}) async-start(), calls=%async_computation.5 | async-start | bytes 3063808 | tf_op jit(solution)/shard_map/all_gather | solution.py:35
  8.2 133.7 %all-gather.10.cloned.1.call-start = ((), (), s32[]{:S(2)}) async-start(), calls=%async_computation.6 | async-start | bytes 4718592 | tf_op jit(solution)/shard_map/all_gather | solution.py:101
  9.0 204.3 %all-gather.12.cloned.1.call-start = ((), (), s32[]{:S(2)}) async-start(), calls=%async_computation.7 | async-start | bytes 12976128 | tf_op jit(solution)/shard_map/all_gather | solution.py:98
  67.2 1.4 copy-start.9
  67.2 1.5 copy-start.10
  67.2 1.6 copy-start.5
  67.2 1.6 copy-start.6
  68.6 217.8 %all-gather.16.cloned.1.call-start = ((), (), s32[]{:S(2)}) async-start(), calls=%async_computation.9 | async-start | bytes 1671168 | tf_op jit(solution)/shard_map/all_gather | solution.py:35
  97.0 49.4 %copy-start.14 = (bf16[2048,704]{0,1:T(8,128)(2,1)S(1)}, bf16[2048,704]{0,1:T(8,128)(2,1)}, u32[]{:S(2)}) copy-start(bf16[2048,704]{0,1:T(8,128)(2,1)} %all-gather.8.cloned.1.call-done) | copy-start | bytes 8650756
  141.9 4.5 copy-start.13
  148.3 4.8 %copy-start.8 = (f32[3,2048]{1,0:T(4,128)S(1)}, f32[3,2048]{1,0:T(4,128)}, u32[]{:S(2)}) copy-start(f32[3,2048]{1,0:T(4,128)} %param.29) | copy-start | bytes 73732
  148.3 64.9 %copy-start.3 = (bf16[128,2048]{1,0:T(8,128)(2,1)S(1)}, bf16[128,2048]{1,0:T(8,128)(2,1)}, u32[]{:S(2)}) copy-start(bf16[128,2048]{1,0:T(8,128)(2,1)} %param.16) | copy-start | bytes 1572868
  149.3 18.6 %all-to-all-start = ((bf16[8,128,352]{1,2,0:T(8,128)(2,1)}), bf16[8,128,352]{1,2,0:T(8,128)(2,1)S(1)}, u32[]{:S(2)}, u32[]{:S(2)}) async-start(bf16[8,128,352]{1,2,0:T(8,128)(2,1)} %bitcast.112), calls=%async_computation | async-start | bytes 1441792 | tf_op jit(solution)/shard_map/all_to_all | solution.py:106
  153.1 178.7 %all-gather.14.cloned.1.call-start = ((), (), s32[]{:S(2)}) async-start(), calls=%async_computation.8 | async-start | bytes 4718592 | tf_op jit(solution)/shard_map/all_gather | solution.py:113
  219.3 1.3 copy-start.7
  221.7 24.6 %all-to-all-start.3 = ((bf16[16,128,128]{1,2,0:T(8,128)(2,1)}), bf16[16,128,128]{1,2,0:T(8,128)(2,1)S(1)}, u32[]{:S(2)}, u32[]{:S(2)}) async-start(bf16[16,128,128]{1,2,0:T(8,128)(2,1)} %broadcast_in_dim.35), calls=%async_computation.3 | async-start | bytes 1048576 | tf_op jit(solution)/shard_map/all_to_all | solution.py:18
  228.8 164.0 %all-gather.18.cloned.1.call-start = ((), (), s32[]{:S(2)}) async-start(), calls=%async_computation.10 | async-start | bytes 4718592 | tf_op jit(solution)/shard_map/all_gather | solution.py:140
  246.3 0.9 copy-start.4
  335.7 4.0 copy-start.11
  335.7 4.0 copy-start.12
  353.9 30.8 %copy-start.15 = (f32[128]{0:T(128)S(1)}, f32[128]{0:T(128)}, u32[]{:S(2)}) copy-start(f32[128]{0:T(128)} %param.27) | copy-start | bytes 1540
  384.7 14.6 %copy-start.1 = (bf16[128,2048]{1,0:T(8,128)(2,1)S(1)}, bf16[128,2048]{1,0:T(8,128)(2,1)}, u32[]{:S(2)}) copy-start(bf16[128,2048]{1,0:T(8,128)(2,1)} %multiply_convert_fusion.2) | copy-start | bytes 1572868
  389.2 10.1 %all-to-all-start.2 = ((bf16[8,128,128]{1,2,0:T(8,128)(2,1)}), bf16[8,128,128]{1,2,0:T(8,128)(2,1)S(1)}, u32[]{:S(2)}, u32[]{:S(2)}) async-start(bf16[8,128,128]{1,2,0:T(8,128)(2,1)} %copy.54), calls=%async_computation.2 | async-start | bytes 524288 | tf_op jit(solution)/shard_map/all_to_all | solution.py:141
  392.8 46.6 %all-gather.20.cloned.1.call-start = ((), (), s32[]{:S(2)}) async-start(), calls=%async_computation.11 | async-start | bytes 4718592 | tf_op jit(solution)/shard_map/all_gather | solution.py:101
  439.3 23.9 %slice-start = ((s8[11534336]{0:T(1024)(128)(4,1)}), s8[4194304]{0:T(1024)(128)(4,1)S(1)}, s32[]{:S(2)}) async-start(s8[11534336]{0:T(1024)(128)(4,1)} %bitcast.141), calls=%async_computation.12 | async-start | bytes 8388608
  439.3 23.9 %slice-start.1 = ((s8[11534336]{0:T(1024)(128)(4,1)}), s8[4194304]{0:T(1024)(128)(4,1)S(1)}, s32[]{:S(2)}) async-start(s8[11534336]{0:T(1024)(128)(4,1)} %bitcast.141), calls=%async_computation.13 | async-start | bytes 8388608
  443.8 19.5 %slice-start.2 = ((s8[11534336]{0:T(1024)(128)(4,1)}), s8[3145728]{0:T(1024)(128)(4,1)S(1)}, s32[]{:S(2)}) async-start(s8[11534336]{0:T(1024)(128)(4,1)} %bitcast.141), calls=%async_computation.14 | async-start | bytes 6291456
  448.4 14.8 %copy-start.2 = (bf16[128,2048]{1,0:T(8,128)(2,1)S(1)}, bf16[128,2048]{1,0:T(8,128)(2,1)}, u32[]{:S(2)}) copy-start(bf16[128,2048]{1,0:T(8,128)(2,1)} %multiply_convert_fusion.1) | copy-start | bytes 1572868
Sparse Core Ops, SparseCore 0:
  9.0 87.9 all-gather.7
  98.9 42.9 all-gather.9
  143.8 69.4 all-gather.11
  214.9 71.4 all-gather.15
  288.1 43.5 all-gather.13
  333.4 38.1 all-gather.17
  404.5 34.8 all-gather.19
where the time goes:
time: 474 us; the launch traced here: 473 us
  waiting for transfers between devices  277 us (58%)
  blocking collectives  71.8 us (15%)
  matrix products  52.6 us (11%)
  other arithmetic  34.7 us (7%)
  starting transfers between devices  14.7 us (3%)
  between operations  13.8 us (3%)
  local copies, waits for them, and re-layouts  8.37 us (2%)
    all_gather x2, waiting for transfers between devices, ffn_half(): gathered = lax.all_gather(current, 'tp', axis=0, tiled=True)  79.9 us
    all_gather x2, waiting for transfers between devices, side_by_side(): result = lax.all_gather(both, axis, axis=dim, tiled=True)  66.6 us
    all_to_all x1, blocking collectives, from_everyone(): return lax.all_to_all(copies, axis, split_axis=0, concat_axis=0, tiled=True)  57.1 us
    all_gather x1, waiting for transfers between devices, on_device(): gathered = lax.all_gather(first, 'tp', axis=0, tiled=True)  45.3 us
    all_gather x1, waiting for transfers between devices, on_device(): down_full = lax.all_gather(down_local, 'tp', axis=0, tiled=True)  45.3 us
    reduce_sum x16, other arithmetic, advance(): jnp.sum(query_blk[:, :, None, :] * key_blk[:, None, :, :] * jnp.exp(log_g...  21.7 us
    all_to_all x1, waiting for transfers between devices, from_everyone(): return lax.all_to_all(copies, axis, split_axis=0, concat_axis=0, tiled=True)  17.3 us
    all_to_all x1, waiting for transfers between devices, ffn_half(): lax.all_to_all(hidden, 'tp', split_axis=0, concat_axis=1, tiled=True)  14.9 us
  transfers between devices with their start and end apart: 10, of which 9 were waited for; matrix products, arithmetic and copies ran while one was open for 16% of the time, Pallas kernels for 0%

commit v1 on v0

--- a/solution.py
+++ b/solution.py
@@ -110,7 +110,14 @@
         )
 
     first = ffn_half(stream, norm_gain[0])
-    gathered = lax.all_gather(first, "tp", axis=0, tiled=True)
+    n_dev_all = lax.axis_size("tp")
+    views = [first]
+    for q in tuple(range(n_dev_all - 1)):
+        views.append(
+            lax.ppermute(views[-1], "tp", [(it, (it + 1) % n_dev_all) for it in range(n_dev_all)])
+        )
+    top = jnp.concatenate(views[::-1], 0)
+    gathered = jnp.roll(top, (lax.axis_index("tp") + 1) * first.shape[0], 0)
     length = gathered.shape[0]
     pieces = side_by_side((query_weight, key_weight, value_weight, outgate_weight), "fs", 0, 1)
     query, key_rows, value_rows, outgate = tuple(

time: 474 us -> 457 us (0.964)
  waiting for transfers between devices: 277 us -> 213 us
  starting transfers between devices: 14.7 us -> 39.8 us
  local copies, waits for them, and re-layouts: 8.37 us -> 28.6 us
    all_gather x1 -> x0, waiting for transfers between devices: 45.3 us -> none  [on_device(): gathered = lax.all_gather(first, 'tp', axis=0, tiled=True)]
    all_gather x2, waiting for transfers between devices: 66.6 us -> 28.5 us  [side_by_side(): result = lax.all_gather(both, axis, axis=dim, tiled=True)]
    ppermute x0 -> x7, waiting for transfers between devices: none -> 30.1 us  [on_device(): lax.ppermute(views[-1], 'tp', [(it, (it + 1) % n_dev_all) for it in range...]
    unnamed x43 -> x65, local copies, waits for them, and re-layouts: 1.67 us -> 22 us
    ppermute x0 -> x7, starting transfers between devices: none -> 12.6 us  [on_device(): lax.ppermute(views[-1], 'tp', [(it, (it + 1) % n_dev_all) for it in range...]
    all_to_all x1, starting transfers between devices: 3.58 us -> 16.1 us  [on_device(): lax.all_to_all(gated, 'tp', split_axis=0, concat_axis=1, tiled=True)]
    all_to_all x1, waiting for transfers between devices: 17.3 us -> 10.5 us  [from_everyone(): return lax.all_to_all(copies, axis, split_axis=0, concat_axis=0, tiled=True)]
  transfers between devices with their start and end apart: 10 -> 16, of which waited for: 9 -> 12; matrix products, arithmetic and copies ran while one was open for 16% -> 20% of each run, Pallas kernels for 0% -> 0%
where the time goes in v1:
time: 457 us; the launch traced here: 456 us
  waiting for transfers between devices  213 us (47%)
  blocking collectives  71.7 us (16%)
  matrix products  52.7 us (12%)
  starting transfers between devices  39.8 us (9%)
  other arithmetic  35.9 us (8%)
  local copies, waits for them, and re-layouts  28.6 us (6%)
  between operations  13.8 us (3%)
    all_gather x2, waiting for transfers between devices, ffn_half(): gathered = lax.all_gather(current, 'tp', axis=0, tiled=True)  76.3 us
    all_to_all x1, blocking collectives, from_everyone(): return lax.all_to_all(copies, axis, split_axis=0, concat_axis=0, tiled=True)  57.1 us
    all_gather x1, waiting for transfers between devices, on_device(): down_full = lax.all_gather(down_local, 'tp', axis=0, tiled=True)  45.1 us
    ppermute x7, waiting for transfers between devices, on_device(): lax.ppermute(views[-1], 'tp', [(it, (it + 1) % n_dev_all) for it in range...  30.1 us
    all_gather x2, waiting for transfers between devices, side_by_side(): result = lax.all_gather(both, axis, axis=dim, tiled=True)  28.5 us
    unnamed x65, local copies, waits for them, and re-layouts  22 us
    reduce_sum x16, other arithmetic, advance(): jnp.sum(query_blk[:, :, None, :] * key_blk[:, None, :, :] * jnp.exp(log_g...  21.7 us
    all_to_all x1, starting transfers between devices, on_device(): lax.all_to_all(gated, 'tp', split_axis=0, concat_axis=1, tiled=True)  16.1 us
  transfers between devices with their start and end apart: 16, of which 12 were waited for; matrix products, arithmetic and copies ran while one was open for 20% of the time, Pallas kernels for 0%

profile of v1, /device:TPU:1, one launch (start us, length us, event | category | flops | bytes accessed | tf_op | source)
XLA Modules:
  0.0 456.0 jit_solution(3742335174867696491)
XLA Ops:
  6.5 1.7 pad_maximum_fusion
  9.0 1.1 broadcast_in_dim.32
  10.1 57.1 %all_to_all.67 = bf16[16,352,128]{2,1,0:T(8,128)(2,1)S(1)} all-to-all(bf16[16,352,128]{2,1,0:T(8,128)(2,1)S(1)} %broadcast_in_dim.32), channel_id=1, replica_groups=mesh['rep'=2,'fs'=16,'tp'=8] {'fs'}, dimensions={0} | all-to-all | bytes 2883584 | tf_op jit(solution)/shard_map/all_to_all | solution.py:18
  67.2 1.3 copy_bitcast_fusion
  68.5 28.5 %all-gather.7.cloned.1.call-done = bf16[2048,704]{0,1:T(8,128)(2,1)} async-done(((bf16[128,704]{0,1:T(8,128)(2,1)}), bf16[2048,704]{0,1:T(8,128)(2,1)}) %all-gather.7.cloned.1.call-update) | async-done | bytes 2883600 | tf_op jit(solution)/shard_map/all_gather | solution.py:35
  97.0 44.9 %all-gather.9.cloned.1.call-done = bf16[1024,2048]{1,0:T(8,128)(2,1)} async-done(((bf16[128,2048]{1,0:T(8,128)(2,1)}), bf16[1024,2048]{1,0:T(8,128)(2,1)}) %all-gather.9.cloned.1.call-update) | async-done | bytes 4194320 | tf_op jit(solution)/shard_map/all_gather | solution.py:101
  141.9 4.5 convolution_bitcast_fusion.2
  146.7 1.8 fusion.45
  149.5 3.7 all-to-all-start
  153.3 15.1 %all-to-all-done = bf16[8,128,352]{1,2,0:T(8,128)(2,1)S(1)} async-done(((bf16[8,128,352]{1,2,0:T(8,128)(2,1)}), bf16[8,128,352]{1,2,0:T(8,128)(2,1)S(1)}, u32[]{:S(2)}, u32[]{:S(2)}) %all-to-all-start) | async-done | bytes 720928 | tf_op jit(solution)/shard_map/all_to_all | solution.py:106
  168.4 45.1 %all-gather.11.cloned.1.call-done = bf16[2816,2048]{1,0:T(8,128)(2,1)} async-done(((bf16[352,2048]{1,0:T(8,128)(2,1)}), bf16[2816,2048]{1,0:T(8,128)(2,1)}) %all-gather.11.cloned.1.call-update) | async-done | bytes 11534352 | tf_op jit(solution)/shard_map/all_gather | solution.py:98
  213.5 6.1 %fusion.103 = (f32[128]{0:T(128)S(1)}, f32[128,2048]{1,0:T(8,128)S(1)}) fusion(bf16[128,2816]{0,1:T(8,128)(2,1)S(1)} %bitcast.143, bf16[2816,2048]{1,0:T(8,128)(2,1)} %all-gather.11.cloned.1.call-done, bf16[128,2048]{1,0:T(8,128)(2,1)S(1)} %copy-done.2), kind=kOutput, calls=%fused_computation.127 | convolution fusion | flops 1477705600 | bytes 13828608 | tf_op jit(solution)/shard_map/dot_general | solution.py:107
  220.1 6.1 %collective-permute-done = bf16[128,2048]{1,0:T(8,128)(2,1)S(1)} collective-permute-done((bf16[128,2048]{1,0:T(8,128)(2,1)S(1)}, bf16[128,2048]{1,0:T(8,128)(2,1)S(1)}, u32[]{:S(2)}, u32[]{:S(2)}) %collective-permute-start) | collective-permute-done | bytes 524320 | tf_op jit(solution)/shard_map/ppermute | solution.py:117
  226.2 2.5 collective-permute-start.1
  229.7 5.1 %collective-permute-done.1 = bf16[128,2048]{1,0:T(8,128)(2,1)S(1)} collective-permute-done((bf16[128,2048]{1,0:T(8,128)(2,1)S(1)}, bf16[128,2048]{1,0:T(8,128)(2,1)S(1)}, u32[]{:S(2)}, u32[]{:S(2)}) %collective-permute-start.1) | collective-permute-done | bytes 524320 | tf_op jit(solution)/shard_map/ppermute | solution.py:117
  234.8 2.5 collective-permute-start.2
  237.3 6.1 %collective-permute-done.2 = bf16[128,2048]{1,0:T(8,128)(2,1)S(1)} collective-permute-done((bf16[128,2048]{1,0:T(8,128)(2,1)S(1)}, bf16[128,2048]{1,0:T(8,128)(2,1)S(1)}, u32[]{:S(2)}, u32[]{:S(2)}) %collective-permute-start.2) | collective-permute-done | bytes 524320 | tf_op jit(solution)/shard_map/ppermute | solution.py:117
  243.4 2.5 collective-permute-start.3
  245.9 6.1 %collective-permute-done.3 = bf16[128,2048]{1,0:T(8,128)(2,1)S(1)} collective-permute-done((bf16[128,2048]{1,0:T(8,128)(2,1)S(1)}, bf16[128,2048]{1,0:T(8,128)(2,1)S(1)}, u32[]{:S(2)}, u32[]{:S(2)}) %collective-permute-start.3) | collective-permute-done | bytes 524320 | tf_op jit(solution)/shard_map/ppermute | solution.py:117
  252.9 2.5 collective-permute-start.4
  255.4 6.6 %collective-permute-done.4 = bf16[128,2048]{1,0:T(8,128)(2,1)} collective-permute-done((bf16[128,2048]{1,0:T(8,128)(2,1)S(1)}, bf16[128,2048]{1,0:T(8,128)(2,1)}, u32[]{:S(2)}, u32[]{:S(2)}) %collective-permute-start.4) | collective-permute-done | bytes 524320 | tf_op jit(solution)/shard_map/ppermute | solution.py:117
  262.0 2.1 collective-permute-start.5
  265.1 7.0 %all-to-all-start.3 = ((bf16[16,128,128]{1,2,0:T(8,128)(2,1)}), bf16[16,128,128]{1,2,0:T(8,128)(2,1)S(1)}, u32[]{:S(2)}, u32[]{:S(2)}) async-start(bf16[16,128,128]{1,2,0:T(8,128)(2,1)} %broadcast_in_dim.35), calls=%async_computation.3 | async-start | bytes 1048576 | tf_op jit(solution)/shard_map/all_to_all | solution.py:18
  273.0 10.5 %all-to-all-done.3 = bf16[16,128,128]{1,2,0:T(8,128)(2,1)S(1)} async-done(((bf16[16,128,128]{1,2,0:T(8,128)(2,1)}), bf16[16,128,128]{1,2,0:T(8,128)(2,1)S(1)}, u32[]{:S(2)}, u32[]{:S(2)}) %all-to-all-start.3) | async-done | bytes 524320 | tf_op jit(solution)/shard_map/all_to_all | solution.py:18
  284.4 1.9 constant_dynamic-update-slice_fusion.15
  286.3 1.9 constant_dynamic-update-slice_fusion.14
  288.2 1.9 constant_dynamic-update-slice_fusion.13
  290.1 1.9 constant_dynamic-update-slice_fusion.12
  295.6 1.9 constant_dynamic-update-slice_fusion.7
  297.5 1.9 constant_dynamic-update-slice_fusion.6
  299.4 1.9 constant_dynamic-update-slice_fusion.5
  305.7 3.8 fusion.93
  309.9 6.3 %fusion.106 = f32[16,1,64,64]{3,0,1,2:T(8,128)S(1)} fusion(f32[16,1,64,64]{3,0,1,2:T(8,128)S(1)} %copy.47), kind=kOutput, calls=%fused_computation.130 | output fusion | flops 4128768 | bytes 524288 | tf_op jit(solution)/shard_map/jit(cumsum)/reduce_window_sum | solution.py:71
  316.3 3.8 fusion.64
  320.3 3.7 fusion.73
  324.2 3.7 fusion.51
  327.9 30.5 %while.13 = (s32[]{:T(128)}, f32[1,64,128]{2,1,0:T(8,128)S(1)}, f32[16,1,64,128]{3,2,1,0:T(8,128)S(1)}, f32[16,1,64,64]{3,0,1,2:T(8,128)S(1)}, f32[16,1,64,64]{3...) while((s32[]{:T(128)}, f32[1,64,128]{2,1,0:T(8,128)S(1)}, ...), condition=%wide.region_5.6_spmd.clone, body=%wide.region_3.5_spmd.clone.sunk | while | flops 4509699 | bytes 544884 | solution.py:73
  328.0 1.4 multiply_reduce_fusion.6
  329.9 1.4 multiply_reduce_fusion.6
  331.8 1.4 multiply_reduce_fusion.6
  333.7 1.4 multiply_reduce_fusion.6
  335.6 1.4 multiply_reduce_fusion.6
  337.5 1.4 multiply_reduce_fusion.6
  339.4 1.4 multiply_reduce_fusion.6
  341.4 1.4 multiply_reduce_fusion.6
  343.3 1.4 multiply_reduce_fusion.6
  345.2 1.4 multiply_reduce_fusion.6
  347.1 1.4 multiply_reduce_fusion.6
  349.0 1.4 multiply_reduce_fusion.6
  350.9 1.4 multiply_reduce_fusion.6
  352.8 1.4 multiply_reduce_fusion.6
  354.7 1.4 multiply_reduce_fusion.6
  356.6 1.4 multiply_reduce_fusion.6
  358.7 3.6 fusion.87
  363.2 16.1 %all-to-all-start.2 = ((bf16[8,128,128]{1,2,0:T(8,128)(2,1)}), bf16[8,128,128]{1,2,0:T(8,128)(2,1)S(1)}, u32[]{:S(2)}, u32[]{:S(2)}) async-start(bf16[8,128,128]{1,2,0:T(8,128)(2,1)} %copy.54), calls=%async_computation.2 | async-start | bytes 524288 | tf_op jit(solution)/shard_map/all_to_all | solution.py:148
  379.3 6.5 %all-to-all-done.2 = bf16[8,128,128]{1,2,0:T(8,128)(2,1)S(1)} async-done(((bf16[8,128,128]{1,2,0:T(8,128)(2,1)}), bf16[8,128,128]{1,2,0:T(8,128)(2,1)S(1)}, u32[]{:S(2)}, u32[]{:S(2)}) %all-to-all-start.2) | async-done | bytes 262176 | tf_op jit(solution)/shard_map/all_to_all | solution.py:148
  385.8 3.8 fusion.104
  389.8 1.0 multiply_convert_fusion.1
  390.9 31.5 %all-gather.17.cloned.1.call-done = bf16[1024,2048]{1,0:T(8,128)(2,1)} async-done(((bf16[128,2048]{1,0:T(8,128)(2,1)}), bf16[1024,2048]{1,0:T(8,128)(2,1)}) %all-gather.17.cloned.1.call-update) | async-done | bytes 4194320 | tf_op jit(solution)/shard_map/all_gather | solution.py:101
  422.3 4.5 fusion.48
  426.8 4.6 %fusion.44 = bf16[44,8,8,128]{3,2,1,0:T(8,128)(2,1)S(1)} fusion(bf16[1024,2048]{1,0:T(8,128)(2,1)} %all-gather.17.cloned.1.call-done, f32[1024,352]{0,1:T(8,128)S(1)} %fusion.48, bf16[2048,704]{0,1:T(8,128)(2,1)} %all-gather.7.cloned.1.call-done), kind=kOutput, calls=%fused_computation.58 | convolution fusion | flops 1478557696 | bytes 7798784 | tf_op jit(solution)/shard_map/dot_general | solution.py:104
  431.6 14.5 %all_to_all.68 = bf16[8,128,352]{1,2,0:T(8,128)(2,1)S(1)} all-to-all(bf16[8,128,352]{1,2,0:T(8,128)(2,1)S(1)} %bitcast.145), channel_id=1, replica_groups=mesh['rep'=2,'fs'=16,'tp'=8] {'tp'}, dimensions={0} | all-to-all | bytes 1441792 | tf_op jit(solution)/shard_map/all_to_all | solution.py:106
  446.1 1.8 fusion.105
  448.2 1.0 multiply_convert_fusion
  (230 shorter events, 26.0 us)
Async XLA Ops:
  6.5 299.1 %copy-start = (bf16[2048,32]{0,1:T(8,128)(2,1)S(1)}, bf16[2048,32]{0,1:T(8,128)(2,1)}, u32[]{:S(2)}) copy-start(bf16[2048,32]{0,1:T(8,128)(2,1)} %param.24) | copy-start | bytes 393220
  6.5 90.5 %all-gather.7.cloned.1.call-start = ((), (), s32[]{:S(2)}) async-start(), calls=%async_computation.5 | async-start | bytes 3063808 | tf_op jit(solution)/shard_map/all_gather | solution.py:35
  8.2 133.7 %all-gather.9.cloned.1.call-start = ((), (), s32[]{:S(2)}) async-start(), calls=%async_computation.6 | async-start | bytes 4718592 | tf_op jit(solution)/shard_map/all_gather | solution.py:101
  9.0 204.5 %all-gather.11.cloned.1.call-start = ((), (), s32[]{:S(2)}) async-start(), calls=%async_computation.7 | async-start | bytes 12976128 | tf_op jit(solution)/shard_map/all_gather | solution.py:98
  141.9 4.5 copy-start.17
  141.9 4.8 %copy-start.18 = (bf16[2048,704]{0,1:T(8,128)(2,1)S(1)}, bf16[2048,704]{0,1:T(8,128)(2,1)}, u32[]{:S(2)}) copy-start(bf16[2048,704]{0,1:T(8,128)(2,1)} %all-gather.7.cloned.1.call-done) | copy-start | bytes 8650756
  146.7 6.6 %copy-start.12 = (f32[3,2048]{1,0:T(4,128)S(1)}, f32[3,2048]{1,0:T(4,128)}, u32[]{:S(2)}) copy-start(f32[3,2048]{1,0:T(4,128)} %param.29) | copy-start | bytes 73732
  146.7 66.8 %copy-start.2 = (bf16[128,2048]{1,0:T(8,128)(2,1)S(1)}, bf16[128,2048]{1,0:T(8,128)(2,1)}, u32[]{:S(2)}) copy-start(bf16[128,2048]{1,0:T(8,128)(2,1)} %param.16) | copy-start | bytes 1572868
  149.5 18.8 %all-to-all-start = ((bf16[8,128,352]{1,2,0:T(8,128)(2,1)}), bf16[8,128,352]{1,2,0:T(8,128)(2,1)S(1)}, u32[]{:S(2)}, u32[]{:S(2)}) async-start(bf16[8,128,352]{1,2,0:T(8,128)(2,1)} %bitcast.107), calls=%async_computation | async-start | bytes 1441792 | tf_op jit(solution)/shard_map/all_to_all | solution.py:106
  153.2 163.0 %all-gather.13.cloned.1.call-start = ((), (), s32[]{:S(2)}) async-start(), calls=%async_computation.8 | async-start | bytes 1671168 | tf_op jit(solution)/shard_map/all_gather | solution.py:35
  213.5 15.3 %copy-start.13 = (bf16[128,64]{0,1:T(8,128)(2,1)S(1)}, bf16[128,64]{0,1:T(8,128)(2,1)}, u32[]{:S(2)}) copy-start(bf16[128,64]{0,1:T(8,128)(2,1)} %param.20) | copy-start | bytes 49156
  213.5 15.4 %copy-start.14 = (bf16[128,64]{0,1:T(8,128)(2,1)S(1)}, bf16[128,64]{0,1:T(8,128)(2,1)}, u32[]{:S(2)}) copy-start(bf16[128,64]{0,1:T(8,128)(2,1)} %param.21) | copy-start | bytes 49156
  213.5 15.5 %copy-start.9 = (bf16[128,128]{1,0:T(8,128)(2,1)S(1)}, bf16[128,128]{1,0:T(8,128)(2,1)}, u32[]{:S(2)}) copy-start(bf16[128,128]{1,0:T(8,128)(2,1)} %param.23) | copy-start | bytes 98308
  213.5 15.5 %copy-start.10 = (bf16[128,128]{1,0:T(8,128)(2,1)S(1)}, bf16[128,128]{1,0:T(8,128)(2,1)}, u32[]{:S(2)}) copy-start(bf16[128,128]{1,0:T(8,128)(2,1)} %param.22) | copy-start | bytes 98308
  213.5 50.6 %copy-start.11 = (bf16[128,128]{1,0:T(8,128)(2,1)S(1)}, bf16[128,128]{1,0:T(8,128)(2,1)}, u32[]{:S(2)}) copy-start(bf16[128,128]{1,0:T(8,128)(2,1)} %param.28) | copy-start | bytes 98308
  220.1 6.1 %collective-permute-start = (bf16[128,2048]{1,0:T(8,128)(2,1)S(1)}, bf16[128,2048]{1,0:T(8,128)(2,1)S(1)}, u32[]{:S(2)}, u32[]{:S(2)}) collective-permute-start(bf16[128,2048]{1,0:T(8,128)(2,1)S(1)} %multiply_convert_fusion.2), channel_id=1, source_target_pairs={{0,1},{1,2},{2,3},{3,4},{4,5},{5,6},{6,7},{7,0},{8,9},{9,10},{10,1... | collective-permute-start | bytes 1572872 | tf_op jit(solution)/shard_map/ppermute | solution.py:117
  226.2 8.6 %collective-permute-start.1 = (bf16[128,2048]{1,0:T(8,128)(2,1)S(1)}, bf16[128,2048]{1,0:T(8,128)(2,1)S(1)}, u32[]{:S(2)}, u32[]{:S(2)}) collective-permute-start(bf16[128,2048]{1,0:T(8,128)(2,1)S(1)} %collective-permute-done), channel_id=1, source_target_pairs={{0,1},{1,2},{2,3},{3,4},{4,5},{5,6},{6,7},{7,0},{8,9},{9,10},{10,1... | collective-permute-start | bytes 1572872 | tf_op jit(solution)/shard_map/ppermute | solution.py:117
  234.8 8.6 %collective-permute-start.2 = (bf16[128,2048]{1,0:T(8,128)(2,1)S(1)}, bf16[128,2048]{1,0:T(8,128)(2,1)S(1)}, u32[]{:S(2)}, u32[]{:S(2)}) collective-permute-start(bf16[128,2048]{1,0:T(8,128)(2,1)S(1)} %collective-permute-done.1), channel_id=1, source_target_pairs={{0,1},{1,2},{2,3},{3,4},{4,5},{5,6},{6,7},{7,0},{8,9},{9,10},{10,1... | collective-permute-start | bytes 1572872 | tf_op jit(solution)/shard_map/ppermute | solution.py:117
  243.4 21.7 %copy-start.4 = (bf16[128,2048]{1,0:T(8,128)(2,1)}, bf16[128,2048]{1,0:T(8,128)(2,1)S(1)}, u32[]{:S(2)}) copy-start(bf16[128,2048]{1,0:T(8,128)(2,1)S(1)} %collective-permute-done.2) | copy-start | bytes 1572868
  243.4 8.6 %collective-permute-start.3 = (bf16[128,2048]{1,0:T(8,128)(2,1)S(1)}, bf16[128,2048]{1,0:T(8,128)(2,1)S(1)}, u32[]{:S(2)}, u32[]{:S(2)}) collective-permute-start(bf16[128,2048]{1,0:T(8,128)(2,1)S(1)} %collective-permute-done.2), channel_id=1, source_target_pairs={{0,1},{1,2},{2,3},{3,4},{4,5},{5,6},{6,7},{7,0},{8,9},{9,10},{10,1... | collective-permute-start | bytes 1572872 | tf_op jit(solution)/shard_map/ppermute | solution.py:117
  252.0 0.8 copy-start.6
  252.9 9.1 %collective-permute-start.4 = (bf16[128,2048]{1,0:T(8,128)(2,1)S(1)}, bf16[128,2048]{1,0:T(8,128)(2,1)}, u32[]{:S(2)}, u32[]{:S(2)}) collective-permute-start(bf16[128,2048]{1,0:T(8,128)(2,1)S(1)} %collective-permute-done.3), channel_id=1, source_target_pairs={{0,1},{1,2},{2,3},{3,4},{4,5},{5,6},{6,7},{7,0},{8,9},{9,10},{10,1... | collective-permute-start | bytes 1572872 | tf_op jit(solution)/shard_map/ppermute | solution.py:117
  262.0 10.4 %collective-permute-start.5 = (bf16[128,2048]{1,0:T(8,128)(2,1)}, bf16[128,2048]{1,0:T(8,128)(2,1)}, u32[]{:S(2)}, u32[]{:S(2)}) collective-permute-start(bf16[128,2048]{1,0:T(8,128)(2,1)} %collective-permute-done.4), channel_id=1, source_target_pairs={{0,1},{1,2},{2,3},{3,4},{4,5},{5,6},{6,7},{7,0},{8,9},{9,10},{10,1... | collective-permute-start | bytes 1572872 | tf_op jit(solution)/shard_map/ppermute | solution.py:117
  265.1 18.4 %all-to-all-start.3 = ((bf16[16,128,128]{1,2,0:T(8,128)(2,1)}), bf16[16,128,128]{1,2,0:T(8,128)(2,1)S(1)}, u32[]{:S(2)}, u32[]{:S(2)}) async-start(bf16[16,128,128]{1,2,0:T(8,128)(2,1)} %broadcast_in_dim.35), calls=%async_computation.3 | async-start | bytes 1048576 | tf_op jit(solution)/shard_map/all_to_all | solution.py:18
  272.2 107.1 %all-gather.15.cloned.1.call-start = ((), (), s32[]{:S(2)}) async-start(), calls=%async_computation.9 | async-start | bytes 4718592 | tf_op jit(solution)/shard_map/all_gather | solution.py:147
  272.4 12.0 %collective-permute-start.6 = (bf16[128,2048]{1,0:T(8,128)(2,1)}, bf16[128,2048]{1,0:T(8,128)(2,1)}, u32[]{:S(2)}, u32[]{:S(2)}) collective-permute-start(bf16[128,2048]{1,0:T(8,128)(2,1)} %collective-permute-done.5), channel_id=1, source_target_pairs={{0,1},{1,2},{2,3},{3,4},{4,5},{5,6},{6,7},{7,0},{8,9},{9,10},{10,1... | collective-permute-start | bytes 1572872 | tf_op jit(solution)/shard_map/ppermute | solution.py:117
  283.5 0.8 copy-start.3
  284.4 7.6 %copy-start.5 = (bf16[128,2048]{1,0:T(8,128)(2,1)S(1)}, bf16[128,2048]{1,0:T(8,128)(2,1)}, u32[]{:S(2)}) copy-start(bf16[128,2048]{1,0:T(8,128)(2,1)} %copy-done.4) | copy-start | bytes 1572868
  292.0 9.2 %copy-start.7 = (bf16[128,2048]{1,0:T(8,128)(2,1)S(1)}, bf16[128,2048]{1,0:T(8,128)(2,1)}, u32[]{:S(2)}) copy-start(bf16[128,2048]{1,0:T(8,128)(2,1)} %copy-done.6) | copy-start | bytes 1572868
  297.5 8.2 %copy-start.15 = (bf16[32,64]{1,0:T(8,128)(2,1)S(1)}, bf16[32,64]{1,0:T(8,128)(2,1)}, u32[]{:S(2)}) copy-start(bf16[32,64]{1,0:T(8,128)(2,1)} %param.25) | copy-start | bytes 12292
  297.5 8.2 %copy-start.16 = (f32[64]{0:T(128)S(1)}, f32[64]{0:T(128)}, u32[]{:S(2)}) copy-start(f32[64]{0:T(128)} %param.26) | copy-start | bytes 772
  324.0 3.9 copy-start.8
  327.9 30.8 %copy-start.19 = (f32[128]{0:T(128)S(1)}, f32[128]{0:T(128)}, u32[]{:S(2)}) copy-start(f32[128]{0:T(128)} %param.27) | copy-start | bytes 1540
  363.2 22.6 %all-to-all-start.2 = ((bf16[8,128,128]{1,2,0:T(8,128)(2,1)}), bf16[8,128,128]{1,2,0:T(8,128)(2,1)S(1)}, u32[]{:S(2)}, u32[]{:S(2)}) async-start(bf16[8,128,128]{1,2,0:T(8,128)(2,1)} %copy.54), calls=%async_computation.2 | async-start | bytes 524288 | tf_op jit(solution)/shard_map/all_to_all | solution.py:148
  379.3 43.0 %all-gather.17.cloned.1.call-start = ((), (), s32[]{:S(2)}) async-start(), calls=%async_computation.10 | async-start | bytes 4718592 | tf_op jit(solution)/shard_map/all_gather | solution.py:101
  422.3 23.8 %slice-start = ((s8[11534336]{0:T(1024)(128)(4,1)}), s8[4194304]{0:T(1024)(128)(4,1)S(1)}, s32[]{:S(2)}) async-start(s8[11534336]{0:T(1024)(128)(4,1)} %bitcast.136), calls=%async_computation.11 | async-start | bytes 8388608
  422.3 23.8 %slice-start.1 = ((s8[11534336]{0:T(1024)(128)(4,1)}), s8[4194304]{0:T(1024)(128)(4,1)S(1)}, s32[]{:S(2)}) async-start(s8[11534336]{0:T(1024)(128)(4,1)} %bitcast.136), calls=%async_computation.12 | async-start | bytes 8388608
  426.8 19.3 %slice-start.2 = ((s8[11534336]{0:T(1024)(128)(4,1)}), s8[3145728]{0:T(1024)(128)(4,1)S(1)}, s32[]{:S(2)}) async-start(s8[11534336]{0:T(1024)(128)(4,1)} %bitcast.136), calls=%async_computation.13 | async-start | bytes 6291456
  426.8 19.3 %copy-start.1 = (bf16[128,2048]{1,0:T(8,128)(2,1)S(1)}, bf16[128,2048]{1,0:T(8,128)(2,1)}, u32[]{:S(2)}) copy-start(bf16[128,2048]{1,0:T(8,128)(2,1)} %multiply_convert_fusion.1) | copy-start | bytes 1572868
Sparse Core Ops, SparseCore 0:
  9.0 87.9 all-gather.6
  98.9 42.9 all-gather.8
  143.8 69.6 all-gather.10
  229.9 74.3 all-gather.12
  305.9 47.0 all-gather.14
  391.0 31.2 all-gather.16
